TPU v7x, 32 devices: a whole 2x2x4 slice. The times are simulated.
32 devices in a mesh: rep: 2 (over x), fs: 8 (over z, y), tp: 2 (over core).
Axes of the slice: x: 2, y: 2, z: 4, core: 2. Of those that a mesh axis runs over, the one named last changes fastest.
Arguments:
- tokens: bfloat16 [256, 16, 2048], P('tp', ('rep', 'fs')), may hold values from -6 to 6
- mix_gain: float32 [2048], replicated, may hold values from 0.1 to 1.9
- value_weight: bfloat16 [2048, 1024], P('fs', 'tp'), may hold values from -0.125 to 0.125
- gate_weight: bfloat16 [2048, 1024], P('fs', 'tp'), may hold values from -0.125 to 0.125
- conv_taps: float32 [31, 1024], P(None, 'tp'), may hold values from -1 to 1
- head_gain: float32 [1024], P('tp'), may hold values from 0.1 to 1.9
- out_weight: bfloat16 [1024, 2048], P('tp', 'fs'), may hold values from -0.1875 to 0.1875
- ffn_gain: float32 [2048], replicated, may hold values from 0.1 to 1.9
- ffn_gate_weight: bfloat16 [2048, 3072], P('fs', 'tp'), may hold values from -0.125 to 0.125
- ffn_up_weight: bfloat16 [2048, 3072], P('fs', 'tp'), may hold values from -0.125 to 0.125
- down_weight: bfloat16 [3072, 2048], P('tp', 'fs'), may hold values from -0.109375 to 0.109375
Outputs:
- layer_out: bfloat16 [256, 16, 2048], P('tp', ('rep', 'fs'))
All inputs are finite; a program needn't handle non-finite values.
Results may differ from a plain program's by a relative error of at most 0.012.
Values may be sent and summed in bfloat16 or wider, within the bound.
A program may use at most 128 MiB of HBM per device.

v0:
```python
import jax
import jax.numpy as jnp
from jax import lax
from jax.sharding import PartitionSpec as P

HEAD_DIM = 128
norm_eps = 1e-06
group_eps = 1e-05


def rms_scale(matrix, scales):
    return matrix * lax.rsqrt(jnp.mean(matrix * matrix, axis=-1, keepdims=True) + norm_eps) * scales


def body(
    tokens,
    mix_gain,
    value_weight,
    gate_weight,
    conv_taps,
    head_gain,
    out_weight,
    ffn_gain,
    ffn_gate_weight,
    ffn_up_weight,
    down_weight,
):
    local_len, seq_count, model_width = tokens.shape
    own_rows = local_len * seq_count
    whole_rows = lax.all_gather(tokens, "tp", axis=0, tiled=True)
    full_len = whole_rows.shape[0]
    normed = rms_scale(whole_rows.reshape(-1, model_width).astype(jnp.float32), mix_gain).astype(
        jnp.bfloat16
    )
    channels = value_weight.shape[1]
    pieces = (
        lax.all_gather(value_weight, "fs", axis=0, tiled=True),
        lax.all_gather(gate_weight, "fs", axis=0, tiled=True),
    )
    sliced = normed
    value_rows = jnp.dot(sliced, pieces[0], preferred_element_type=jnp.float32)
    gate_rows = jnp.dot(sliced, pieces[1], preferred_element_type=jnp.float32)
    glu_rows = (
        (value_rows * jax.nn.sigmoid(gate_rows))
        .astype(jnp.bfloat16)
        .reshape(full_len, seq_count, channels)
    )
    kernel = conv_taps.shape[0]
    conved = lax.conv_general_dilated(
        glu_rows.astype(jnp.float32),
        conv_taps[:, None, :],
        (1,),
        [(kernel // 2, kernel // 2)],
        dimension_numbers=("WNC", "WIO", "WNC"),
        feature_group_count=channels,
        precision=lax.Precision.HIGHEST,
    )
    grouped = conved.reshape(full_len, seq_count, channels // HEAD_DIM, HEAD_DIM)
    head_mean = jnp.mean(grouped, axis=-1, keepdims=True)
    head_var = jnp.mean(jnp.square(grouped - head_mean), axis=-1, keepdims=True)
    scaled = (
        (grouped - head_mean) * lax.rsqrt(head_var + group_eps) * head_gain.reshape(-1, HEAD_DIM)
    )
    activated = jax.nn.silu(scaled).astype(jnp.bfloat16).reshape(-1, channels)
    out_columns = lax.all_gather(out_weight, "fs", axis=1, tiled=True)
    sliced = lax.slice_in_dim(activated, 0, own_rows * lax.axis_size("tp"), axis=0)
    mixed_rows = lax.psum_scatter(
        jnp.dot(sliced, out_columns, preferred_element_type=jnp.float32).astype(jnp.bfloat16),
        "tp",
        scatter_dimension=0,
        tiled=True,
    ).astype(jnp.float32)
    residual = tokens.reshape(own_rows, model_width).astype(jnp.float32)
    middle = (residual + mixed_rows).astype(jnp.bfloat16)
    middle_whole = lax.all_gather(
        middle.reshape(local_len, seq_count, model_width), "tp", axis=0, tiled=True
    )
    normed_ffn = rms_scale(
        middle_whole.reshape(-1, model_width).astype(jnp.float32), ffn_gain
    ).astype(jnp.bfloat16)
    pieces = (
        lax.all_gather(ffn_gate_weight, "fs", axis=0, tiled=True),
        lax.all_gather(ffn_up_weight, "fs", axis=0, tiled=True),
    )
    sliced = normed_ffn
    gate_part = jnp.dot(sliced, pieces[0], preferred_element_type=jnp.float32)
    up_part = jnp.dot(sliced, pieces[1], preferred_element_type=jnp.float32)
    hidden = (jax.nn.silu(gate_part) * up_part).astype(jnp.bfloat16)
    down_columns = lax.all_gather(down_weight, "fs", axis=1, tiled=True)
    sliced = hidden
    fed_rows = lax.psum_scatter(
        jnp.dot(sliced, down_columns, preferred_element_type=jnp.float32).astype(jnp.bfloat16),
        "tp",
        scatter_dimension=0,
        tiled=True,
    ).astype(jnp.float32)
    layer_rows = (middle.astype(jnp.float32) + fed_rows).astype(jnp.bfloat16)
    return layer_rows.reshape(local_len, seq_count, model_width)


def solution(mesh):
    placed = (
        P("tp", ("rep", "fs"), None),
        P(),
        P("fs", "tp"),
        P("fs", "tp"),
        P(None, "tp"),
        P("tp"),
        P("tp", "fs"),
        P(),
        P("fs", "tp"),
        P("fs", "tp"),
        P("tp", "fs"),
    )
    return jax.shard_map(
        body, mesh=mesh, in_specs=placed, out_specs=P("tp", ("rep", "fs"), None), check_vma=False
    )
```

profile of v0, /device:TPU:0, one launch (start us, length us, event | category | flops | bytes accessed | tf_op | source)
XLA Modules:
  0.0 522.6 jit_solution(14361909878251636009)
XLA Ops:
  6.5 0.7 all-gather.10.cloned.1.call-update
  7.3 0.7 all-gather.14.cloned.1.call-update
  8.1 0.7 all-gather.12.cloned.1.call-update
  8.8 0.5 all-gather.16.cloned.1.call-update
  9.4 11.3 %all-gather.10.cloned.1.call-done = bf16[256,1,2048]{2,0,1:T(8,128)(2,1)} async-done(((bf16[128,1,2048]{2,0,1:T(8,128)(2,1)}), bf16[256,1,2048]{2,0,1:T(8,128)(2,1)}) %all-gather.10.cloned.1.call-update) | async-done | bytes 1048592 | tf_op jit(solution)/shard_map/all_gather | solution.py:30
  20.7 1.5 fusion.4
  22.2 50.9 %all-gather.14.cloned.1.call-done = bf16[2048,512]{1,0:T(8,128)(2,1)} async-done(((bf16[256,512]{1,0:T(8,128)(2,1)}), bf16[2048,512]{1,0:T(8,128)(2,1)}) %all-gather.14.cloned.1.call-update) | async-done | bytes 2097168 | tf_op jit(solution)/shard_map/all_gather | solution.py:38
  73.1 2.8 fusion.9
  75.8 47.0 %all-gather.12.cloned.1.call-done = bf16[2048,512]{1,0:T(8,128)(2,1)} async-done(((bf16[256,512]{1,0:T(8,128)(2,1)}), bf16[2048,512]{1,0:T(8,128)(2,1)}) %all-gather.12.cloned.1.call-update) | async-done | bytes 2097168 | tf_op jit(solution)/shard_map/all_gather | solution.py:37
  122.9 2.3 fusion.11
  125.5 0.4 copy-done.8
  125.9 1.3 convolution_select_fusion
  127.2 0.3 copy.19
  128.1 0.3 reduce_sum.37
  128.4 0.6 multiply_reduce_fusion
  129.1 44.6 %all-gather.16.cloned.1.call-done = bf16[512,2048]{1,0:T(8,128)(2,1)} async-done(((bf16[512,256]{1,0:T(8,128)(2,1)}), bf16[512,2048]{1,0:T(8,128)(2,1)}) %all-gather.16.cloned.1.call-update) | async-done | bytes 2097168 | tf_op jit(solution)/shard_map/all_gather | solution.py:65
  174.0 0.3 sub.31
  174.4 3.4 convolution_convert_fusion
  177.8 6.7 %reduce-scatter.3.cloned.1.call-done = bf16[128,2048]{1,0:T(8,128)(2,1)} async-done(((bf16[256,2048]{1,0:T(8,128)(2,1)}), bf16[128,2048]{1,0:T(8,128)(2,1)}) %reduce-scatter.3.cloned.1.call-update) | async-done | bytes 524304 | tf_op jit(solution)/shard_map/reduce_scatter | solution.py:67
  184.5 2.0 fusion.13
  186.5 0.7 all-gather.18.cloned.1.call-update
  187.3 0.7 all-gather.20.cloned.1.call-update
  188.0 0.7 all-gather.22.cloned.1.call-update
  188.8 8.1 %all-gather.24.cloned.1.call-done = bf16[256,2048]{1,0:T(8,128)(2,1)} async-done(((bf16[128,2048]{1,0:T(8,128)(2,1)}), bf16[256,2048]{1,0:T(8,128)(2,1)}) %all-gather.24.cloned.1.call-update) | async-done | bytes 1048592 | tf_op jit(solution)/shard_map/all_gather | solution.py:75
  196.9 1.5 fusion.3
  198.4 100.6 %all-gather.18.cloned.1.call-done = bf16[2048,1536]{1,0:T(8,128)(2,1)} async-done(((bf16[256,1536]{1,0:T(8,128)(2,1)}), bf16[2048,1536]{1,0:T(8,128)(2,1)}) %all-gather.18.cloned.1.call-update) | async-done | bytes 6291472 | tf_op jit(solution)/shard_map/all_gather | solution.py:82
  299.0 5.0 fusion.26
  303.9 94.1 %all-gather.20.cloned.1.call-done = bf16[2048,1536]{1,0:T(8,128)(2,1)} async-done(((bf16[256,1536]{1,0:T(8,128)(2,1)}), bf16[2048,1536]{1,0:T(8,128)(2,1)}) %all-gather.20.cloned.1.call-update) | async-done | bytes 6291472 | tf_op jit(solution)/shard_map/all_gather | solution.py:83
  398.1 99.7 %all-gather.22.cloned.1.call-done = bf16[1536,2048]{1,0:T(8,128)(2,1)} async-done(((bf16[1536,256]{1,0:T(8,128)(2,1)}), bf16[1536,2048]{1,0:T(8,128)(2,1)}) %all-gather.22.cloned.1.call-update) | async-done | bytes 6291472 | tf_op jit(solution)/shard_map/all_gather | solution.py:89
  497.8 9.3 %convolution_convert_fusion.1 = bf16[256,2048]{1,0:T(8,128)(2,1)} fusion(bf16[1536,2048]{1,0:T(8,128)(2,1)} %all-gather.22.cloned.1.call-done, bf16[2048,1536]{1,0:T(8,128)(2,1)} %all-gather.20.cloned.1.call-done, f32[256,1536]{1,0:T(8,128)S(1)} %fusion.26, bf16[256,2048]{1,0:T(8,128)(2,1)S(1)} %copy-done.3, f32[2048]{0:T(1024)S(1)} %copy-done.6, ...), kind=kOutput, calls=%fused_computation.7 | convolution fusion | flops 3226206208 | bytes 16262144 | tf_op jit(solution)/shard_map/dot_general | solution.py:92
  507.1 6.7 %reduce-scatter.5.cloned.1.call-done = bf16[128,2048]{1,0:T(8,128)(2,1)} async-done(((bf16[256,2048]{1,0:T(8,128)(2,1)}), bf16[128,2048]{1,0:T(8,128)(2,1)}) %reduce-scatter.5.cloned.1.call-update) | async-done | bytes 524304 | tf_op jit(solution)/shard_map/reduce_scatter | solution.py:91
  513.8 2.0 fusion.20
  (43 shorter events, 1.6 us)
Async XLA Ops:
  6.5 119.0 %copy-start = (f32[31,512]{1,0:T(8,128)S(1)}, f32[31,512]{1,0:T(8,128)}, u32[]{:S(2)}) copy-start(f32[31,512]{1,0:T(8,128)} %param.15) | copy-start | bytes 190468
  6.5 66.5 %copy-start.5 = (f32[2048]{0:T(1024)S(1)}, f32[2048]{0:T(1024)}, u32[]{:S(2)}) copy-start(f32[2048]{0:T(1024)} %param.12) | copy-start | bytes 24580
  6.5 14.1 %all-gather.10.cloned.1.call-start = ((), (), s32[]{:S(2)}) async-start(), calls=%async_computation.2 | async-start | bytes 1572864 | tf_op jit(solution)/shard_map/all_gather | solution.py:30
  7.3 65.8 %all-gather.14.cloned.1.call-start = ((), (), s32[]{:S(2)}) async-start(), calls=%async_computation.4 | async-start | bytes 2359296 | tf_op jit(solution)/shard_map/all_gather | solution.py:38
  8.0 114.9 %all-gather.12.cloned.1.call-start = ((), (), s32[]{:S(2)}) async-start(), calls=%async_computation.3 | async-start | bytes 2359296 | tf_op jit(solution)/shard_map/all_gather | solution.py:37
  8.7 164.9 %all-gather.16.cloned.1.call-start = ((), (), s32[]{:S(2)}) async-start(), calls=%async_computation.5 | async-start | bytes 2359296 | tf_op jit(solution)/shard_map/all_gather | solution.py:65
  9.3 175.2 %reduce-scatter.3.cloned.1.call-start = ((), (), s32[]{:S(2)}) async-start(), calls=%async_computation.6 | async-start | bytes 1572864 | tf_op jit(solution)/shard_map/reduce_scatter | solution.py:67
  22.2 100.7 %copy-start.4 = (bf16[256,1,2048]{2,0,1:T(8,128)(2,1)S(1)}, bf16[256,1,2048]{2,0,1:T(8,128)(2,1)}, u32[]{:S(2)}) copy-start(bf16[256,1,2048]{2,0,1:T(8,128)(2,1)} %all-gather.10.cloned.1.call-done) | copy-start | bytes 3145732
  125.2 0.7 copy-start.8
  127.8 46.5 %copy-start.7 = (f32[512]{0:T(512)S(1)}, f32[512]{0:T(512)}, u32[]{:S(2)}) copy-start(f32[512]{0:T(512)} %param.16) | copy-start | bytes 6148
  174.3 10.2 %copy-start.2 = (bf16[128,1,2048]{2,0,1:T(8,128)(2,1)S(1)}, bf16[128,1,2048]{2,0,1:T(8,128)(2,1)}, u32[]{:S(2)}) copy-start(bf16[128,1,2048]{2,0,1:T(8,128)(2,1)} %param.11) | copy-start | bytes 1572868
  177.8 19.1 %all-gather.24.cloned.1.call-start = ((), (), s32[]{:S(2)}) async-start(), calls=%async_computation.11 | async-start | bytes 1572864 | tf_op jit(solution)/shard_map/all_gather | solution.py:75
  186.5 112.5 %copy-start.6 = (f32[2048]{0:T(1024)S(1)}, f32[2048]{0:T(1024)}, u32[]{:S(2)}) copy-start(f32[2048]{0:T(1024)} %param.18) | copy-start | bytes 24580
  186.5 112.5 %all-gather.18.cloned.1.call-start = ((), (), s32[]{:S(2)}) async-start(), calls=%async_computation.7 | async-start | bytes 7077888 | tf_op jit(solution)/shard_map/all_gather | solution.py:82
  187.2 210.8 %all-gather.20.cloned.1.call-start = ((), (), s32[]{:S(2)}) async-start(), calls=%async_computation.8 | async-start | bytes 7077888 | tf_op jit(solution)/shard_map/all_gather | solution.py:83
  188.0 309.8 %all-gather.22.cloned.1.call-start = ((), (), s32[]{:S(2)}) async-start(), calls=%async_computation.9 | async-start | bytes 7077888 | tf_op jit(solution)/shard_map/all_gather | solution.py:89
  188.7 325.1 %reduce-scatter.5.cloned.1.call-start = ((), (), s32[]{:S(2)}) async-start(), calls=%async_computation.10 | async-start | bytes 1572864 | tf_op jit(solution)/shard_map/reduce_scatter | solution.py:91
  198.4 299.4 %copy-start.3 = (bf16[256,2048]{1,0:T(8,128)(2,1)S(1)}, bf16[256,2048]{1,0:T(8,128)(2,1)}, u32[]{:S(2)}) copy-start(bf16[256,2048]{1,0:T(8,128)(2,1)} %all-gather.24.cloned.1.call-done) | copy-start | bytes 3145732
  303.9 209.9 %copy-start.1 = (bf16[128,2048]{1,0:T(8,128)(2,1)S(1)}, bf16[128,2048]{1,0:T(8,128)(2,1)}, u32[]{:S(2)}) copy-start(bf16[128,2048]{1,0:T(8,128)(2,1)} %fusion.13) | copy-start | bytes 1572868
Sparse Core Ops, SparseCore 0:
  8.9 11.7 all-gather.9
  22.8 50.2 all-gather.13
  75.2 47.6 all-gather.11
  124.8 48.8 all-gather.15
  177.9 6.5 reduce-scatter.2
  186.6 10.2 all-gather.23
  199.1 99.8 all-gather.17
  301.1 96.8 all-gather.19
  400.1 97.6 all-gather.21
  507.2 6.5 reduce-scatter.4
where the time goes:
time: 523 us
  waiting for transfers between devices  474 us (91%)
  matrix products  24 us (5%)
  between operations  13.7 us (3%)
  other arithmetic  7.98 us (2%)
    all_gather x1, waiting for transfers between devices, body(): lax.all_gather(ffn_gate_weight, 'fs', axis=0, tiled=True)  101 us
    all_gather x1, waiting for transfers between devices, body(): down_columns = lax.all_gather(down_weight, 'fs', axis=1, tiled=True)  99.7 us
    all_gather x1, waiting for transfers between devices, body(): lax.all_gather(ffn_up_weight, 'fs', axis=0, tiled=True)  94.1 us
    all_gather x1, waiting for transfers between devices, body(): lax.all_gather(gate_weight, 'fs', axis=0, tiled=True)  50.9 us
    all_gather x1, waiting for transfers between devices, body(): lax.all_gather(value_weight, 'fs', axis=0, tiled=True)  47 us
    all_gather x1, waiting for transfers between devices, body(): out_columns = lax.all_gather(out_weight, 'fs', axis=1, tiled=True)  44.6 us
    all_gather x1, waiting for transfers between devices, body(): whole_rows = lax.all_gather(tokens, 'tp', axis=0, tiled=True)  11.3 us
  transfers between devices with their start and end apart: 10, of which 10 were waited for; matrix products, arithmetic and copies ran while one was open for 3% of the time, Pallas kernels for 0%

commit v1 on v0

--- a/solution.py
+++ b/solution.py
@@ -6,6 +6,21 @@
 HEAD_DIM = 128
 norm_eps = 1e-06
 group_eps = 1e-05
+
+
+def proceed_trees_for(vec):
+    width = jax.lax.axis_size("fs")
+    z = [(c - 1, c) for c in range(1, width)] + [(width - 1, 0)]
+    local_now = vec
+    copies = [local_now]
+    idx = 0
+    while idx < width - 1:
+        local_now = jax.lax.ppermute(local_now, "fs", z)
+        copies += [local_now]
+        idx += 1
+    x_now = jnp.concatenate([*reversed(copies)], axis=1)
+    z_new = jnp.roll(x_now, (jax.lax.axis_index("fs") + 1) * local_now.shape[1], axis=1)
+    return z_new
 
 
 def rms_scale(matrix, scales):
@@ -62,7 +77,7 @@
         (grouped - head_mean) * lax.rsqrt(head_var + group_eps) * head_gain.reshape(-1, HEAD_DIM)
     )
     activated = jax.nn.silu(scaled).astype(jnp.bfloat16).reshape(-1, channels)
-    out_columns = lax.all_gather(out_weight, "fs", axis=1, tiled=True)
+    out_columns = proceed_trees_for(out_weight)
     sliced = lax.slice_in_dim(activated, 0, own_rows * lax.axis_size("tp"), axis=0)
     mixed_rows = lax.psum_scatter(
         jnp.dot(sliced, out_columns, preferred_element_type=jnp.float32).astype(jnp.bfloat16),

time: 523 us -> 493 us (0.943)
  waiting for transfers between devices: 474 us -> 430 us
  local copies, waits for them, and re-layouts: 2.15 us -> 13.8 us
    ppermute x0 -> x7, waiting for transfers between devices: none -> 83.6 us  [proceed_trees_for(): local_now = jax.lax.ppermute(local_now, 'fs', z)]
    all_gather x1, waiting for transfers between devices: 50.9 us -> 0.01 us  [body(): lax.all_gather(gate_weight, 'fs', axis=0, tiled=True)]
    all_gather x1 -> x0, waiting for transfers between devices: 44.6 us -> none  [body(): out_columns = lax.all_gather(out_weight, 'fs', axis=1, tiled=True)]
    all_gather x1, waiting for transfers between devices: 47 us -> 26.6 us  [body(): lax.all_gather(value_weight, 'fs', axis=0, tiled=True)]
    all_gather x1, waiting for transfers between devices: 11.3 us -> 0.01 us  [body(): whole_rows = lax.all_gather(tokens, 'tp', axis=0, tiled=True)]
    unnamed x18 -> x35, local copies, waits for them, and re-layouts: 0.41 us -> 11.3 us
  transfers between devices with their start and end apart: 10 -> 16, of which waited for: 10 -> 14; matrix products, arithmetic and copies ran while one was open for 3% -> 5% of each run, Pallas kernels for 0% -> 0%
where the time goes in v1:
time: 493 us; the launch traced here: 492 us
  waiting for transfers between devices  430 us (87%)
  matrix products  23.7 us (5%)
  local copies, waits for them, and re-layouts  13.8 us (3%)
  between operations  13.4 us (3%)
  other arithmetic  7.97 us (2%)
    all_gather x1, waiting for transfers between devices, body(): lax.all_gather(ffn_gate_weight, 'fs', axis=0, tiled=True)  100 us
    all_gather x1, waiting for transfers between devices, body(): down_columns = lax.all_gather(down_weight, 'fs', axis=1, tiled=True)  99.7 us
    all_gather x1, waiting for transfers between devices, body(): lax.all_gather(ffn_up_weight, 'fs', axis=0, tiled=True)  94.1 us
    ppermute x7, waiting for transfers between devices, proceed_trees_for(): local_now = jax.lax.ppermute(local_now, 'fs', z)  83.6 us
    all_gather x1, waiting for transfers between devices, body(): lax.all_gather(value_weight, 'fs', axis=0, tiled=True)  26.6 us
    unnamed x35, local copies, waits for them, and re-layouts  11.3 us
  transfers between devices with their start and end apart: 16, of which 14 were waited for; matrix products, arithmetic and copies ran while one was open for 5% of the time, Pallas kernels for 0%

profile of v1, /device:TPU:0, one launch (start us, length us, event | category | flops | bytes accessed | tf_op | source)
XLA Modules:
  0.0 492.1 jit_solution(1834050734006623645)
XLA Ops:
  8.1 3.0 collective-permute-start
  11.1 9.6 %collective-permute-done = bf16[512,256]{1,0:T(8,128)(2,1)S(1)} collective-permute-done((bf16[512,256]{1,0:T(8,128)(2,1)}, bf16[512,256]{1,0:T(8,128)(2,1)S(1)}, u32[]{:S(2)}, u32[]{:S(2)}) %collective-permute-start) | collective-permute-done | bytes 262176 | tf_op jit(solution)/shard_map/ppermute | solution.py:18
  20.7 10.2 %collective-permute-done.1 = bf16[512,256]{1,0:T(8,128)(2,1)S(1)} collective-permute-done((bf16[512,256]{1,0:T(8,128)(2,1)S(1)}, bf16[512,256]{1,0:T(8,128)(2,1)S(1)}, u32[]{:S(2)}, u32[]{:S(2)}) %collective-permute-start.1) | collective-permute-done | bytes 262176 | tf_op jit(solution)/shard_map/ppermute | solution.py:18
  30.9 15.0 %collective-permute-done.2 = bf16[512,256]{1,0:T(8,128)(2,1)S(1)} collective-permute-done((bf16[512,256]{1,0:T(8,128)(2,1)S(1)}, bf16[512,256]{1,0:T(8,128)(2,1)S(1)}, u32[]{:S(2)}, u32[]{:S(2)}) %collective-permute-start.2) | collective-permute-done | bytes 262176 | tf_op jit(solution)/shard_map/ppermute | solution.py:18
  45.9 9.1 %collective-permute-done.3 = bf16[512,256]{1,0:T(8,128)(2,1)S(1)} collective-permute-done((bf16[512,256]{1,0:T(8,128)(2,1)S(1)}, bf16[512,256]{1,0:T(8,128)(2,1)S(1)}, u32[]{:S(2)}, u32[]{:S(2)}) %collective-permute-start.3) | collective-permute-done | bytes 262176 | tf_op jit(solution)/shard_map/ppermute | solution.py:18
  55.0 16.4 %collective-permute-done.4 = bf16[512,256]{1,0:T(8,128)(2,1)S(1)} collective-permute-done((bf16[512,256]{1,0:T(8,128)(2,1)S(1)}, bf16[512,256]{1,0:T(8,128)(2,1)S(1)}, u32[]{:S(2)}, u32[]{:S(2)}) %collective-permute-start.4) | collective-permute-done | bytes 262176 | tf_op jit(solution)/shard_map/ppermute | solution.py:18
  71.3 15.9 %collective-permute-done.5 = bf16[512,256]{1,0:T(8,128)(2,1)S(1)} collective-permute-done((bf16[512,256]{1,0:T(8,128)(2,1)S(1)}, bf16[512,256]{1,0:T(8,128)(2,1)S(1)}, u32[]{:S(2)}, u32[]{:S(2)}) %collective-permute-start.5) | collective-permute-done | bytes 262176 | tf_op jit(solution)/shard_map/ppermute | solution.py:18
  87.3 1.5 fusion.4
  88.8 7.5 %collective-permute-done.6 = bf16[512,256]{1,0:T(8,128)(2,1)S(1)} collective-permute-done((bf16[512,256]{1,0:T(8,128)(2,1)S(1)}, bf16[512,256]{1,0:T(8,128)(2,1)S(1)}, u32[]{:S(2)}, u32[]{:S(2)}) %collective-permute-start.6) | collective-permute-done | bytes 262176 | tf_op jit(solution)/shard_map/ppermute | solution.py:18
  97.8 0.8 constant_dynamic-update-slice_fusion.13
  99.3 0.8 constant_dynamic-update-slice_fusion.11
  101.6 0.8 constant_dynamic-update-slice_fusion.8
  103.1 0.8 constant_dynamic-update-slice_fusion.6
  103.9 0.8 constant_dynamic-update-slice_fusion.5
  104.6 0.8 constant_dynamic-update-slice_fusion.4
  105.4 0.8 constant_dynamic-update-slice_fusion.3
  108.4 2.4 fusion.10
  110.8 26.6 %all-gather.11.cloned.1.call-done = bf16[2048,512]{1,0:T(8,128)(2,1)} async-done(((bf16[256,512]{1,0:T(8,128)(2,1)}), bf16[2048,512]{1,0:T(8,128)(2,1)}) %all-gather.11.cloned.1.call-update) | async-done | bytes 2097168 | tf_op jit(solution)/shard_map/all_gather | solution.py:52
  137.4 2.3 fusion.12
  140.1 1.3 convolution_select_fusion
  143.9 3.4 convolution_convert_fusion
  147.4 7.0 %reduce-scatter.3.cloned.1.call-done = bf16[128,2048]{1,0:T(8,128)(2,1)} async-done(((bf16[256,2048]{1,0:T(8,128)(2,1)}), bf16[128,2048]{1,0:T(8,128)(2,1)}) %reduce-scatter.3.cloned.1.call-update) | async-done | bytes 524304 | tf_op jit(solution)/shard_map/reduce_scatter | solution.py:82
  154.4 2.0 fusion.14
  158.7 8.1 %all-gather.21.cloned.1.call-done = bf16[256,2048]{1,0:T(8,128)(2,1)} async-done(((bf16[128,2048]{1,0:T(8,128)(2,1)}), bf16[256,2048]{1,0:T(8,128)(2,1)}) %all-gather.21.cloned.1.call-update) | async-done | bytes 1048592 | tf_op jit(solution)/shard_map/all_gather | solution.py:90
  166.8 1.5 fusion.3
  168.3 100.4 %all-gather.15.cloned.1.call-done = bf16[2048,1536]{1,0:T(8,128)(2,1)} async-done(((bf16[256,1536]{1,0:T(8,128)(2,1)}), bf16[2048,1536]{1,0:T(8,128)(2,1)}) %all-gather.15.cloned.1.call-update) | async-done | bytes 6291472 | tf_op jit(solution)/shard_map/all_gather | solution.py:97
  268.8 5.0 %fusion.27 = f32[256,1536]{1,0:T(8,128)S(1)} fusion(bf16[2048,1536]{1,0:T(8,128)(2,1)} %all-gather.15.cloned.1.call-done, bf16[256,2048]{1,0:T(8,128)(2,1)} %all-gather.21.cloned.1.call-done, f32[2048]{0:T(1024)S(1)} %copy-done.7, f32[256]{0:T(256)S(1)} %add_rsqrt_fusion.1), kind=kOutput, calls=%fused_computation.39 | convolution fusion | flops 1612709888 | bytes 8922112 | tf_op jit(solution)/shard_map/dot_general | solution.py:101
  273.7 94.1 %all-gather.17.cloned.1.call-done = bf16[2048,1536]{1,0:T(8,128)(2,1)} async-done(((bf16[256,1536]{1,0:T(8,128)(2,1)}), bf16[2048,1536]{1,0:T(8,128)(2,1)}) %all-gather.17.cloned.1.call-update) | async-done | bytes 6291472 | tf_op jit(solution)/shard_map/all_gather | solution.py:98
  367.8 99.7 %all-gather.19.cloned.1.call-done = bf16[1536,2048]{1,0:T(8,128)(2,1)} async-done(((bf16[1536,256]{1,0:T(8,128)(2,1)}), bf16[1536,2048]{1,0:T(8,128)(2,1)}) %all-gather.19.cloned.1.call-update) | async-done | bytes 6291472 | tf_op jit(solution)/shard_map/all_gather | solution.py:104
  467.6 9.3 %convolution_convert_fusion.1 = bf16[256,2048]{1,0:T(8,128)(2,1)} fusion(bf16[1536,2048]{1,0:T(8,128)(2,1)} %all-gather.19.cloned.1.call-done, bf16[2048,1536]{1,0:T(8,128)(2,1)} %all-gather.17.cloned.1.call-done, f32[256,1536]{1,0:T(8,128)S(1)} %fusion.27, bf16[256,2048]{1,0:T(8,128)(2,1)S(1)} %copy-done.4, f32[2048]{0:T(1024)S(1)} %copy-done.7, ...), kind=kOutput, calls=%fused_computation.7 | convolution fusion | flops 3226206208 | bytes 16262144 | tf_op jit(solution)/shard_map/dot_general | solution.py:107
  476.9 6.7 %reduce-scatter.5.cloned.1.call-done = bf16[128,2048]{1,0:T(8,128)(2,1)} async-done(((bf16[256,2048]{1,0:T(8,128)(2,1)}), bf16[128,2048]{1,0:T(8,128)(2,1)}) %reduce-scatter.5.cloned.1.call-update) | async-done | bytes 524304 | tf_op jit(solution)/shard_map/reduce_scatter | solution.py:106
  483.6 2.0 fusion.21
  (72 shorter events, 13.3 us)
Async XLA Ops:
  6.5 133.5 %copy-start = (f32[31,512]{1,0:T(8,128)S(1)}, f32[31,512]{1,0:T(8,128)}, u32[]{:S(2)}) copy-start(f32[31,512]{1,0:T(8,128)} %param.15) | copy-start | bytes 190468
  6.5 95.0 %copy-start.5 = (bf16[512,256]{1,0:T(8,128)(2,1)S(1)}, bf16[512,256]{1,0:T(8,128)(2,1)}, u32[]{:S(2)}) copy-start(bf16[512,256]{1,0:T(8,128)(2,1)} %param.17) | copy-start | bytes 786436
  6.5 80.7 %all-gather.9.cloned.1.call-start = ((), (), s32[]{:S(2)}) async-start(), calls=%async_computation.2 | async-start | bytes 1572864 | tf_op jit(solution)/shard_map/all_gather | solution.py:45
  7.3 101.1 %all-gather.13.cloned.1.call-start = ((), (), s32[]{:S(2)}) async-start(), calls=%async_computation.4 | async-start | bytes 2359296 | tf_op jit(solution)/shard_map/all_gather | solution.py:53
  8.0 129.4 %all-gather.11.cloned.1.call-start = ((), (), s32[]{:S(2)}) async-start(), calls=%async_computation.3 | async-start | bytes 2359296 | tf_op jit(solution)/shard_map/all_gather | solution.py:52
  8.1 12.6 %collective-permute-start = (bf16[512,256]{1,0:T(8,128)(2,1)}, bf16[512,256]{1,0:T(8,128)(2,1)S(1)}, u32[]{:S(2)}, u32[]{:S(2)}) collective-permute-start(bf16[512,256]{1,0:T(8,128)(2,1)} %param.17), channel_id=1, source_target_pairs={{0,2},{2,4},{4,6},{6,8},{8,10},{10,12},{12,14},{14,0},{1,3},{3,5},... | collective-permute-start | bytes 786440 | tf_op jit(solution)/shard_map/ppermute | solution.py:18
  20.7 10.2 %collective-permute-start.1 = (bf16[512,256]{1,0:T(8,128)(2,1)S(1)}, bf16[512,256]{1,0:T(8,128)(2,1)S(1)}, u32[]{:S(2)}, u32[]{:S(2)}) collective-permute-start(bf16[512,256]{1,0:T(8,128)(2,1)S(1)} %collective-permute-done), channel_id=1, source_target_pairs={{0,2},{2,4},{4,6},{6,8},{8,10},{10,12},{12,14},{14,0},{1,3},{3,5},... | collective-permute-start | bytes 786440 | tf_op jit(solution)/shard_map/ppermute | solution.py:18
  30.8 15.1 %collective-permute-start.2 = (bf16[512,256]{1,0:T(8,128)(2,1)S(1)}, bf16[512,256]{1,0:T(8,128)(2,1)S(1)}, u32[]{:S(2)}, u32[]{:S(2)}) collective-permute-start(bf16[512,256]{1,0:T(8,128)(2,1)S(1)} %collective-permute-done.1), channel_id=1, source_target_pairs={{0,2},{2,4},{4,6},{6,8},{8,10},{10,12},{12,14},{14,0},{1,3},{3,5},... | collective-permute-start | bytes 786440 | tf_op jit(solution)/shard_map/ppermute | solution.py:18
  30.9 123.5 %reduce-scatter.3.cloned.1.call-start = ((), (), s32[]{:S(2)}) async-start(), calls=%async_computation.5 | async-start | bytes 1572864 | tf_op jit(solution)/shard_map/reduce_scatter | solution.py:82
  45.9 9.1 %collective-permute-start.3 = (bf16[512,256]{1,0:T(8,128)(2,1)S(1)}, bf16[512,256]{1,0:T(8,128)(2,1)S(1)}, u32[]{:S(2)}, u32[]{:S(2)}) collective-permute-start(bf16[512,256]{1,0:T(8,128)(2,1)S(1)} %collective-permute-done.2), channel_id=1, source_target_pairs={{0,2},{2,4},{4,6},{6,8},{8,10},{10,12},{12,14},{14,0},{1,3},{3,5},... | collective-permute-start | bytes 786440 | tf_op jit(solution)/shard_map/ppermute | solution.py:18
  55.0 16.4 %collective-permute-start.4 = (bf16[512,256]{1,0:T(8,128)(2,1)S(1)}, bf16[512,256]{1,0:T(8,128)(2,1)S(1)}, u32[]{:S(2)}, u32[]{:S(2)}) collective-permute-start(bf16[512,256]{1,0:T(8,128)(2,1)S(1)} %collective-permute-done.3), channel_id=1, source_target_pairs={{0,2},{2,4},{4,6},{6,8},{8,10},{10,12},{12,14},{14,0},{1,3},{3,5},... | collective-permute-start | bytes 786440 | tf_op jit(solution)/shard_map/ppermute | solution.py:18
  71.3 15.9 %collective-permute-start.5 = (bf16[512,256]{1,0:T(8,128)(2,1)S(1)}, bf16[512,256]{1,0:T(8,128)(2,1)S(1)}, u32[]{:S(2)}, u32[]{:S(2)}) collective-permute-start(bf16[512,256]{1,0:T(8,128)(2,1)S(1)} %collective-permute-done.4), channel_id=1, source_target_pairs={{0,2},{2,4},{4,6},{6,8},{8,10},{10,12},{12,14},{14,0},{1,3},{3,5},... | collective-permute-start | bytes 786440 | tf_op jit(solution)/shard_map/ppermute | solution.py:18
  87.3 9.1 %collective-permute-start.6 = (bf16[512,256]{1,0:T(8,128)(2,1)S(1)}, bf16[512,256]{1,0:T(8,128)(2,1)S(1)}, u32[]{:S(2)}, u32[]{:S(2)}) collective-permute-start(bf16[512,256]{1,0:T(8,128)(2,1)S(1)} %collective-permute-done.5), channel_id=1, source_target_pairs={{0,2},{2,4},{4,6},{6,8},{8,10},{10,12},{12,14},{14,0},{1,3},{3,5},... | collective-permute-start | bytes 786440 | tf_op jit(solution)/shard_map/ppermute | solution.py:18
  88.8 19.6 %copy-start.3 = (bf16[256,1,2048]{2,0,1:T(8,128)(2,1)S(1)}, bf16[256,1,2048]{2,0,1:T(8,128)(2,1)}, u32[]{:S(2)}) copy-start(bf16[256,1,2048]{2,0,1:T(8,128)(2,1)} %all-gather.9.cloned.1.call-done) | copy-start | bytes 3145732
  88.8 19.6 %copy-start.6 = (f32[2048]{0:T(1024)S(1)}, f32[2048]{0:T(1024)}, u32[]{:S(2)}) copy-start(f32[2048]{0:T(1024)} %param.12) | copy-start | bytes 24580
  110.8 29.3 %copy-start.9 = (pred[8,36]{0,1:T(8,128)(4,1)S(1)}, pred[8,36]{0,1:T(8,128)(4,1)}, u32[]{:S(2)}) copy-start(pred[8,36]{0,1:T(8,128)(4,1)} %constant.59) | copy-start | bytes 868
  141.3 2.6 copy-start.8
  143.2 11.2 %copy-start.2 = (bf16[128,1,2048]{2,0,1:T(8,128)(2,1)S(1)}, bf16[128,1,2048]{2,0,1:T(8,128)(2,1)}, u32[]{:S(2)}) copy-start(bf16[128,1,2048]{2,0,1:T(8,128)(2,1)} %param.11) | copy-start | bytes 1572868
  147.3 121.4 %copy-start.7 = (f32[2048]{0:T(1024)S(1)}, f32[2048]{0:T(1024)}, u32[]{:S(2)}) copy-start(f32[2048]{0:T(1024)} %param.18) | copy-start | bytes 24580
  147.3 19.5 %all-gather.21.cloned.1.call-start = ((), (), s32[]{:S(2)}) async-start(), calls=%async_computation.10 | async-start | bytes 1572864 | tf_op jit(solution)/shard_map/all_gather | solution.py:90
  156.4 112.4 %all-gather.15.cloned.1.call-start = ((), (), s32[]{:S(2)}) async-start(), calls=%async_computation.6 | async-start | bytes 7077888 | tf_op jit(solution)/shard_map/all_gather | solution.py:97
  157.0 210.9 %all-gather.17.cloned.1.call-start = ((), (), s32[]{:S(2)}) async-start(), calls=%async_computation.7 | async-start | bytes 7077888 | tf_op jit(solution)/shard_map/all_gather | solution.py:98
  157.7 309.9 %all-gather.19.cloned.1.call-start = ((), (), s32[]{:S(2)}) async-start(), calls=%async_computation.8 | async-start | bytes 7077888 | tf_op jit(solution)/shard_map/all_gather | solution.py:104
  158.5 325.2 %reduce-scatter.5.cloned.1.call-start = ((), (), s32[]{:S(2)}) async-start(), calls=%async_computation.9 | async-start | bytes 1572864 | tf_op jit(solution)/shard_map/reduce_scatter | solution.py:106
  168.3 299.2 %copy-start.4 = (bf16[256,2048]{1,0:T(8,128)(2,1)S(1)}, bf16[256,2048]{1,0:T(8,128)(2,1)}, u32[]{:S(2)}) copy-start(bf16[256,2048]{1,0:T(8,128)(2,1)} %all-gather.21.cloned.1.call-done) | copy-start | bytes 3145732
  273.7 209.9 %copy-start.1 = (bf16[128,2048]{1,0:T(8,128)(2,1)S(1)}, bf16[128,2048]{1,0:T(8,128)(2,1)}, u32[]{:S(2)}) copy-start(bf16[128,2048]{1,0:T(8,128)(2,1)} %fusion.14) | copy-start | bytes 1572868
Sparse Core Ops, SparseCore 0:
  8.9 11.7 all-gather.8
  22.8 60.3 all-gather.12
  85.3 52.0 all-gather.10
  147.5 6.8 reduce-scatter.2
  156.5 10.2 all-gather.20
  168.8 99.8 all-gather.14
  270.9 96.8 all-gather.16
  369.9 97.6 all-gather.18
  477.0 6.5 reduce-scatter.4
